TPU v7x, 32 devices: a whole 2x2x4 slice. The times are simulated.
32 devices in a mesh: sp: 4 (over z), dp: 8 (over y, x, core).
Axes of the slice: x: 2, y: 2, z: 4, core: 2. Of those that a mesh axis runs over, the one named last changes fastest.
Arguments:
- queries: bfloat16 [8, 768, 6144], P('dp', None, 'sp'), may hold values from -64 to 64
- out_grad: bfloat16 [8, 768, 4096], P('dp', None, 'sp'), may hold values from -6 to 6
- latent: bfloat16 [8, 768, 512], P('dp'), may hold values from -6 to 6
- rope_key: bfloat16 [8, 768, 64], P('dp'), may hold values from -6 to 6
- kv_gain: float32 [512], replicated, may hold values from 0.1 to 1.9
- key_up: bfloat16 [512, 4096], P('dp', 'sp'), may hold values from -0.25 to 0.25
- value_up: bfloat16 [512, 4096], P('dp', 'sp'), may hold values from -0.25 to 0.25
Outputs:
- query_grad: bfloat16 [8, 768, 6144], P('dp', None, 'sp')
- latent_grad: bfloat16 [8, 768, 512], P('dp')
- rope_key_grad: bfloat16 [8, 768, 64], P('dp')
- key_up_grad: float32 [512, 4096], P('dp', 'sp')
- value_up_grad: float32 [512, 4096], P('dp', 'sp')
All inputs are finite; a program needn't handle non-finite values.
Results may differ from a plain program's by a relative error of at most 0.019.
The roundings to bfloat16 on the way count: a program that leaves them out, or rounds other values in their place, can miss the bound.
Values may be sent and summed in bfloat16 or wider, within the bound.
A program may use at most 64 MiB of HBM per device.

v0:
```python
import jax
import jax.numpy as jnp
from jax import lax
from jax.sharding import PartitionSpec as P

NOPE_DIM = 128
ROPE_DIM = 64
VALUE_DIM = 128


norm_eps = 1e-06
rope_theta = 10000.0


def rope_tables(length, width):
    half_width = width // 2
    frequency = rope_theta ** (-(jnp.arange(half_width, dtype=jnp.float32) * 2.0 / width))
    position = jnp.arange(length, dtype=jnp.int32).astype(jnp.float32)
    angles = position[:, None] * frequency[None, :]
    return (jnp.cos(angles), jnp.sin(angles))


def rotate(tensor, cosine, sine_table):
    half_width = tensor.shape[-1] // 2
    first_half = tensor[..., :half_width]
    second = tensor[..., half_width:]
    return jnp.concatenate(
        [first_half * cosine - second * sine_table, second * cosine + first_half * sine_table],
        axis=-1,
    )


def unrotate(upstream, cosine, sine_table):
    half_width = upstream.shape[-1] // 2
    first_half = upstream[..., :half_width]
    second = upstream[..., half_width:]
    return jnp.concatenate(
        [first_half * cosine + second * sine_table, second * cosine - first_half * sine_table],
        axis=-1,
    )


def head_backward(query_used, key_used, head_value, head_grad, score_scale):
    length = query_used.shape[0]
    scores = jnp.dot(query_used, key_used.T, preferred_element_type=jnp.float32) * score_scale
    causal = lax.broadcasted_iota(jnp.int32, (length, length), 0) >= lax.broadcasted_iota(
        jnp.int32, (length, length), 1
    )
    scores = jnp.where(causal, scores, -jnp.inf)
    row_top = jnp.max(scores, axis=1, keepdims=True)
    weights = jnp.exp(scores - row_top)
    probs = weights / jnp.sum(weights, axis=1, keepdims=True)
    probs_low = probs.astype(jnp.bfloat16)
    value_grad = jnp.dot(probs_low.T, head_grad, preferred_element_type=jnp.float32).astype(
        jnp.bfloat16
    )
    prob_grad = jnp.dot(head_grad, head_value.T, preferred_element_type=jnp.float32)
    center = jnp.sum(probs * prob_grad, axis=1, keepdims=True)
    score_grad = (probs * (prob_grad - center) * score_scale).astype(jnp.bfloat16)
    query_grad = jnp.dot(score_grad, key_used, preferred_element_type=jnp.float32)
    key_grad = jnp.dot(score_grad.T, query_used, preferred_element_type=jnp.float32)
    return (query_grad, key_grad, value_grad)


def attend(queries, head_grads, keys, values, key_rot, cosine, sine_table):
    length = queries.shape[0]
    head_count = head_grads.shape[1] // VALUE_DIM
    qk_width = NOPE_DIM + ROPE_DIM
    query_heads = queries.reshape(length, head_count, qk_width)
    rotated = rotate(
        query_heads[:, :, NOPE_DIM:].astype(jnp.float32), cosine[:, None, :], sine_table[:, None, :]
    ).astype(jnp.bfloat16)
    query_used = jnp.concatenate([query_heads[:, :, :NOPE_DIM], rotated], axis=-1).transpose(
        1, 0, 2
    )
    key_heads = keys.reshape(length, head_count, NOPE_DIM).transpose(1, 0, 2)
    key_used = jnp.concatenate(
        [key_heads, jnp.broadcast_to(key_rot[None], (head_count, length, ROPE_DIM))], axis=-1
    )
    value_heads = values.reshape(length, head_count, VALUE_DIM).transpose(1, 0, 2)
    grad_heads = head_grads.reshape(length, head_count, VALUE_DIM).transpose(1, 0, 2)
    score_scale = qk_width ** (-0.5)
    query_part, key_part, value_part = lax.map(
        lambda items: head_backward(items[0], items[1], items[2], items[3], score_scale),
        (query_used, key_used, value_heads, grad_heads),
    )
    query_rot_grad = unrotate(query_part[:, :, NOPE_DIM:], cosine[None], sine_table[None])
    query_grad = jnp.concatenate([query_part[:, :, :NOPE_DIM], query_rot_grad], axis=-1).astype(
        jnp.bfloat16
    )
    query_grad = query_grad.transpose(1, 0, 2).reshape(length, head_count * qk_width)
    key_plain_grad = (
        key_part[:, :, :NOPE_DIM]
        .astype(jnp.bfloat16)
        .transpose(1, 0, 2)
        .reshape(length, head_count * NOPE_DIM)
    )
    key_rot_grad = jnp.sum(key_part[:, :, NOPE_DIM:], axis=0)
    value_grad = value_part.transpose(1, 0, 2).reshape(length, head_count * VALUE_DIM)
    return (query_grad, key_plain_grad, key_rot_grad, value_grad)


def finish(comp_total, rot_total, raw_latent, inverse, kv_gain, cosine, sine_table):
    mixed = comp_total * kv_gain
    spread = jnp.mean(raw_latent * mixed, axis=-1, keepdims=True)
    latent_grad = (inverse * mixed - raw_latent * inverse**3 * spread).astype(jnp.bfloat16)
    rope_grad = unrotate(rot_total, cosine, sine_table).astype(jnp.bfloat16)
    return (latent_grad, rope_grad)


def shards(queries, out_grad, latent, rope_key, kv_gain, key_up, value_up):
    key_whole, value_whole = (
        lax.all_gather(key_up, "dp", axis=0, tiled=True),
        lax.all_gather(value_up, "dp", axis=0, tiled=True),
    )
    batch_count, seq_count, latent_width = latent.shape
    raw_latent = latent.astype(jnp.float32)
    inverse = lax.rsqrt(jnp.mean(raw_latent * raw_latent, axis=-1, keepdims=True) + norm_eps)
    compressed = (raw_latent * inverse * kv_gain).astype(jnp.bfloat16)
    cosine, sine_table = rope_tables(seq_count, ROPE_DIM)
    key_rot = rotate(rope_key.astype(jnp.float32), cosine, sine_table).astype(jnp.bfloat16)
    flat_comp = compressed.reshape(batch_count * seq_count, latent_width)
    keys = jnp.dot(flat_comp, key_whole, preferred_element_type=jnp.float32).astype(jnp.bfloat16)
    values = jnp.dot(flat_comp, value_whole, preferred_element_type=jnp.float32).astype(
        jnp.bfloat16
    )
    keys = keys.reshape(batch_count, seq_count, key_whole.shape[1])
    values = values.reshape(batch_count, seq_count, value_whole.shape[1])

    def per_sequence(items):
        query_grad, key_plain_grad, key_rot_grad, value_grad = attend(
            items[0], items[1], items[2], items[3], items[4], cosine, sine_table
        )
        comp_part = jnp.dot(
            key_plain_grad, key_whole.T, preferred_element_type=jnp.float32
        ) + jnp.dot(value_grad, value_whole.T, preferred_element_type=jnp.float32)
        return (query_grad, key_plain_grad, value_grad, comp_part, key_rot_grad)

    query_grad, key_plain_grad, value_grad, comp_part, rot_part = lax.map(
        per_sequence, (queries, out_grad, keys, values, key_rot)
    )
    grad_pair = jnp.concatenate([key_plain_grad, value_grad], axis=-1).reshape(
        batch_count * seq_count, -1
    )
    grad_scale = float(lax.axis_size("dp") * batch_count * seq_count) ** (-0.5)
    comp_total = lax.psum(comp_part.astype(jnp.bfloat16), "sp").astype(jnp.float32)
    rot_total = lax.psum(rot_part.astype(jnp.bfloat16), "sp").astype(jnp.float32)
    latent_grad, rope_grad = finish(
        comp_total, rot_total, raw_latent, inverse, kv_gain, cosine, sine_table
    )
    product = lax.dot_general(
        flat_comp, grad_pair, (((0,), (0,)), ((), ())), preferred_element_type=jnp.float32
    )
    combined = lax.psum_scatter(product * grad_scale, "dp", scatter_dimension=0, tiled=True)
    split_at = key_up.shape[1]
    return (query_grad, latent_grad, rope_grad, combined[:, :split_at], combined[:, split_at:])


def solution(mesh):
    return jax.shard_map(
        shards,
        mesh=mesh,
        in_specs=(
            P("dp", None, "sp"),
            P("dp", None, "sp"),
            P("dp", None, None),
            P("dp", None, None),
            P(),
            P("dp", "sp"),
            P("dp", "sp"),
        ),
        out_specs=(
            P("dp", None, "sp"),
            P("dp", None, None),
            P("dp", None, None),
            P("dp", "sp"),
            P("dp", "sp"),
        ),
        check_vma=False,
    )
```

profile of v0, /device:TPU:24, one launch (start us, length us, event | category | flops | bytes accessed | tf_op | source)
XLA Modules:
  0.0 270.2 jit_solution(8573621979364724312)
XLA Ops:
  10.3 2.6 copy.21
  12.9 2.8 %copy.18 = bf16[1,768,1536]{1,2,0:T(8,128)(2,1)S(1)} copy(bf16[1,768,1536]{2,1,0:T(8,128)(2,1)} %param.9) | data formatting | bytes 4718592 | tf_op args[0]
  15.9 1.0 copy-done
  18.2 1.6 maximum_bitcast_fusion.2
  19.8 14.5 %all-gather.5.cloned.1.call-done = bf16[512,1024]{1,0:T(8,128)(2,1)} async-done(((bf16[64,1024]{1,0:T(8,128)(2,1)}), bf16[512,1024]{1,0:T(8,128)(2,1)}) %all-gather.5.cloned.1.call-update) | async-done | bytes 1048592 | tf_op jit(solution)/shard_map/all_gather | solution.py:114
  34.2 2.3 fusion.43
  36.5 1.4 copy.35
  38.0 21.6 %all-gather.3.cloned.1.call-done = bf16[512,1024]{1,0:T(8,128)(2,1)} async-done(((bf16[64,1024]{1,0:T(8,128)(2,1)}), bf16[512,1024]{1,0:T(8,128)(2,1)}) %all-gather.3.cloned.1.call-update) | async-done | bytes 1048592 | tf_op jit(solution)/shard_map/all_gather | solution.py:113
  59.5 2.3 fusion.42
  62.3 2.3 pad_maximum_fusion
  64.6 88.8 %while.19 = (s32[]{:T(128)}, f32[8,768,192]{1,2,0:T(8,128)}, f32[8,768,192]{1,2,0:T(8,128)}, bf16[8,768,128]{1,2,0:T(8,128)(2,1)}, bf16[8,768,192]{1,2,0:T(8,128...) while((s32[]{:T(128)}, f32[8,768,192]{1,2,0:T(8,128)}, ...), condition=%wide.region_5.6_spmd, body=%wide.region_1.5_spmd.sunk | while | flops 992769792 | bytes 24220780 | solution.py:83
  64.6 1.6 fusion.96
  66.6 1.4 fusion.100
  68.9 1.6 multiply_reduce_fusion.2
  71.1 2.3 fusion.99
  73.5 2.3 fusion.98
  75.7 1.6 fusion.96
  77.7 1.4 fusion.100
  80.0 1.6 multiply_reduce_fusion.2
  82.2 2.4 fusion.99
  84.5 2.2 fusion.98
  86.8 1.6 fusion.96
  88.7 1.4 fusion.100
  91.0 1.6 multiply_reduce_fusion.2
  93.2 2.3 fusion.99
  95.6 2.3 fusion.98
  97.9 1.6 fusion.96
  99.8 1.4 fusion.100
  102.1 1.6 multiply_reduce_fusion.2
  104.4 2.4 fusion.99
  106.7 2.3 fusion.98
  109.0 1.6 fusion.96
  111.0 1.4 fusion.100
  113.3 1.6 multiply_reduce_fusion.2
  115.5 2.3 fusion.99
  117.8 2.3 fusion.98
  120.1 1.6 fusion.96
  122.0 1.4 fusion.100
  124.3 1.6 multiply_reduce_fusion.2
  126.5 2.4 fusion.99
  128.9 2.2 fusion.98
  131.2 1.6 fusion.96
  133.1 1.4 fusion.100
  135.4 1.6 multiply_reduce_fusion.2
  137.6 2.4 fusion.99
  140.0 2.3 fusion.98
  142.3 1.6 fusion.96
  144.2 1.4 fusion.100
  146.5 1.6 multiply_reduce_fusion.2
  148.7 2.4 fusion.99
  151.1 2.3 fusion.98
  153.4 2.2 slice_reduce_fusion
  155.6 2.1 slice.115
  157.7 1.0 fusion.70
  159.4 1.9 fusion.44
  161.6 5.5 %convolution_multiply_fusion = f32[512,2048]{1,0:T(8,128)} fusion(bf16[1,768,1024]{1,2,0:T(8,128)(2,1)} %bitcast.133, bf16[1,768,1024]{1,2,0:T(8,128)(2,1)S(1)} %bitcast.131, bf16[1,768,512]{2,1,0:T(8,128)(2,1)S(1)} %copy-done, f32[512]{0:T(512)S(1)} %copy-done.9, f32[768]{0:T(1024)S(1)} %copy-done.7), kind=kOutput, calls=%fused_computation.36 | convolution fusion | flops 1619525632 | bytes 8131584 | tf_op jit(solution)/shard_map/dot_general | solution.py:151
  167.1 2.1 slice.116
  169.3 1.6 add_convert_fusion.1
  171.1 2.4 copy.26
  173.5 32.9 %all-reduce.3.cloned.1.call-done = (bf16[1,768,512]{2,1,0:T(8,128)(2,1)}, bf16[1,768,64]{1,2,0:T(8,128)(2,1)}) async-done(((bf16[1,768,512]{2,1,0:T(8,128)(2,1)}, bf16[1,768,64]{1,2,0:T(8,128)(2,1)}), (bf16[1,768,512]{2,1,0:T(8,128)(2,1)}, bf16[1,768,64]{1,2,0:T(8,128)(2,1)})) %all-reduce.3.cloned.1.call-update) | async-done | bytes 884752 | tf_op jit(solution)/shard_map/psum | solution.py:146
  208.5 1.5 fusion.41
  210.0 1.3 fusion.40
  211.3 50.4 %reduce-scatter.2.cloned.1.call-done = f32[64,2048]{1,0:T(8,128)} async-done(((f32[512,2048]{1,0:T(8,128)}), f32[64,2048]{1,0:T(8,128)}) %reduce-scatter.2.cloned.1.call-update) | async-done | bytes 524304 | tf_op jit(solution)/shard_map/reduce_scatter | solution.py:154
  261.8 1.9 fusion.69
  (91 shorter events, 22.6 us)
Async XLA Ops:
  7.2 27.1 %all-gather.5.cloned.1.call-start = ((), (), s32[]{:S(2)}) async-start(), calls=%async_computation.2 | async-start | bytes 1179648 | tf_op jit(solution)/shard_map/all_gather | solution.py:114
  7.9 51.6 %all-gather.3.cloned.1.call-start = ((), (), s32[]{:S(2)}) async-start(), calls=%async_computation.1 | async-start | bytes 1179648 | tf_op jit(solution)/shard_map/all_gather | solution.py:113
  8.6 197.8 %all-reduce.3.cloned.1.call-start = ((), (), s32[]{:S(2)}) async-start(), calls=%async_computation.4 | async-start | bytes 1769472 | tf_op jit(solution)/shard_map/psum | solution.py:146
  8.7 8.4 %copy-start.10 = (f32[32]{0:T(128)}, f32[32]{0:T(128)S(1)}, u32[]{:S(2)}) copy-start(f32[32]{0:T(128)S(1)} %negate_power_fusion) | copy-start | bytes 388
  15.7 1.1 copy-start
  17.5 0.6 copy-start.2
  17.5 0.7 copy-start.4
  18.2 16.1 %copy-start.8 = (f32[512]{0:T(512)S(1)}, f32[512]{0:T(512)}, u32[]{:S(2)}) copy-start(f32[512]{0:T(512)} %param.13) | copy-start | bytes 6148
  19.8 39.8 %copy-start.6 = (f32[768]{0:T(1024)}, f32[768]{0:T(1024)S(1)}, u32[]{:S(2)}) copy-start(f32[768]{0:T(1024)S(1)} %get-tuple-element.145) | copy-start | bytes 9220
  153.4 4.3 %copy-start.14 = (bf16[512,1024]{1,0:T(8,128)(2,1)S(1)}, bf16[512,1024]{1,0:T(8,128)(2,1)}, u32[]{:S(2)}) copy-start(bf16[512,1024]{1,0:T(8,128)(2,1)} %all-gather.3.cloned.1.call-done) | copy-start | bytes 3145732
  157.7 1.4 copy-start.12
  157.7 1.7 copy-start.13
  159.4 2.2 copy-start.7
  159.4 2.2 copy-start.9
  161.3 100.4 %reduce-scatter.2.cloned.1.call-start = ((), (), s32[]{:S(2)}) async-start(), calls=%async_computation.3 | async-start | bytes 4718592 | tf_op jit(solution)/shard_map/reduce_scatter | solution.py:154
  167.1 2.2 copy-start.3
  167.1 2.1 copy-start.5
  171.1 36.4 %copy-start.11 = (f32[32]{0:T(128)S(1)}, f32[32]{0:T(128)}, u32[]{:S(2)}) copy-start(f32[32]{0:T(128)} %copy-done.10) | copy-start | bytes 388
  206.4 3.6 %copy-start.1 = (bf16[1,768,512]{2,1,0:T(8,128)(2,1)S(1)}, bf16[1,768,512]{2,1,0:T(8,128)(2,1)}, u32[]{:S(2)}) copy-start(bf16[1,768,512]{2,1,0:T(8,128)(2,1)} %get-tuple-element.126) | copy-start | bytes 2359300
Sparse Core Ops, SparseCore 0:
  9.9 24.3 all-gather.4
  36.1 23.3 all-gather.2
  161.4 44.9 all-reduce.2
  209.7 52.0 reduce-scatter.1
where the time goes:
time: 274 us; the launch traced here: 270 us
  waiting for transfers between devices  121 us (44%)
  matrix products  87 us (32%)
  local copies, waits for them, and re-layouts  24.8 us (9%)
  other arithmetic  22.9 us (8%)
  between operations  14.1 us (5%)
    reduce_scatter x1, waiting for transfers between devices, shards(): lax.psum_scatter(product * grad_scale, 'dp', scatter_dimension=0, tiled=T...  50.4 us
    psum x1, waiting for transfers between devices, shards(): lax.psum(comp_part.astype(jnp.bfloat16), 'sp').astype(jnp.float32)  32.9 us
    all_gather x1, waiting for transfers between devices, shards(): lax.all_gather(key_up, 'dp', axis=0, tiled=True)  21.6 us
    dot_general x8, matrix products, head_backward(): jnp.dot(score_grad.T, query_used, preferred_element_type=jnp.float32)  18.9 us
    dot_general x8, matrix products, head_backward(): jnp.dot(score_grad, key_used, preferred_element_type=jnp.float32)  18.1 us
    all_gather x1, waiting for transfers between devices, shards(): lax.all_gather(value_up, 'dp', axis=0, tiled=True)  14.5 us
    dot_general x8, matrix products, head_backward(): jnp.dot(head_grad, head_value.T, preferred_element_type=jnp.float32)  12.8 us
    dot_general x8, matrix products, head_backward(): jnp.dot(query_used, key_used.T, preferred_element_type=jnp.float32)  12.7 us
  transfers between devices with their start and end apart: 4, of which 4 were waited for; matrix products, arithmetic and copies ran while one was open for 11% of the time, Pallas kernels for 0%

commit v1 on v0

v1 whole, which is shorter than its diff:
```python
import functools

import jax
import jax.numpy as jnp
import numpy as np
from jax import lax
from jax.experimental import pallas as pl
from jax.experimental.pallas import tpu as pltpu
from jax.sharding import PartitionSpec as P

NOPE_DIM = 128
ROPE_DIM = 64
VALUE_DIM = 128
QK = NOPE_DIM + ROPE_DIM
LOG2E = 1.4426950408889634

norm_eps = 1e-06
rope_theta = 10000.0

NT = (((1,), (1,)), ((), ()))


def rope_tables(length):
    half = ROPE_DIM // 2
    frequency = np.float32(rope_theta) ** (-(np.arange(half, dtype=np.float32) * np.float32(2.0 / ROPE_DIM)))
    angles = np.arange(length, dtype=np.float32)[:, None] * frequency.astype(np.float32)[None, :]
    return np.cos(angles).astype(np.float32), np.sin(angles).astype(np.float32)


def dot(a, b):
    return jnp.dot(a, b, preferred_element_type=jnp.float32)


def dot_nt(a, b):
    return lax.dot_general(a, b, NT, preferred_element_type=jnp.float32)


def swap_halves(x):
    lane = lax.broadcasted_iota(jnp.int32, x.shape, 1)
    return jnp.where(lane % ROPE_DIM < ROPE_DIM // 2, pltpu.roll(x, 96, 1), pltpu.roll(x, 32, 1))


def attention_kernel(
    block, grad_scale,
    latent_ref, rope_ref, gain_ref, cos_ref, sin_ref, cos_t_ref, sin_t_ref,
    q_ref, do_ref, wk_ref, wv_ref,
    dq_ref, dw_ref, part_ref, rot_ref,
    comp, comp_t, krot, krot_t, ku, kt, vals, qu, pt, dst, dkv, acc, rot_acc,
):
    step = pl.program_id(0)
    length = q_ref.shape[0]
    tiles = length // block
    scale = QK ** (-0.5)

    @pl.when(step == 0)
    def _():
        raw = latent_ref[...].astype(jnp.float32)
        inverse = lax.rsqrt(jnp.mean(raw * raw, axis=-1, keepdims=True) + norm_eps)
        normed = raw * inverse * gain_ref[...]
        comp[...] = normed.astype(jnp.bfloat16)
        comp_t[...] = normed.T.astype(jnp.bfloat16)
        rope = rope_ref[...].astype(jnp.float32)
        wide = jnp.concatenate([rope, rope], axis=1)
        turned = wide * cos_ref[...] + swap_halves(wide) * sin_ref[...]
        krot[...] = turned.astype(jnp.bfloat16)
        krot_t[...] = turned.T.astype(jnp.bfloat16)
        acc[...] = jnp.zeros_like(acc)
        rot_acc[...] = jnp.zeros_like(rot_acc)

    keys = dot(comp[...], wk_ref[...])
    keys_t = keys.T.astype(jnp.bfloat16)
    keys = keys.astype(jnp.bfloat16)
    vals[...] = dot(comp[...], wv_ref[...]).astype(jnp.bfloat16)
    for h in range(2):
        ku[h, :, :NOPE_DIM] = keys[:, h * NOPE_DIM:(h + 1) * NOPE_DIM]
        ku[h, :, NOPE_DIM:] = krot[:, :ROPE_DIM]
        kt[h, :NOPE_DIM, :] = keys_t[h * NOPE_DIM:(h + 1) * NOPE_DIM, :]
        kt[h, NOPE_DIM:, :] = krot_t[:ROPE_DIM, :]

    mid = q_ref[:, 128:256].astype(jnp.float32)
    last = q_ref[:, 256:384].astype(jnp.float32)
    low = lax.broadcasted_iota(jnp.int32, mid.shape, 1) < 64
    plain = jnp.where(low, pltpu.roll(mid, 64, 1), pltpu.roll(last, 64, 1))
    rope = jnp.where(low, mid, last)
    turned = rope * cos_ref[...] + swap_halves(rope) * sin_ref[...]
    qu[0, :, :NOPE_DIM] = q_ref[:, :128]
    qu[0, :, NOPE_DIM:] = turned[:, :ROPE_DIM].astype(jnp.bfloat16)
    qu[1, :, :NOPE_DIM] = plain.astype(jnp.bfloat16)
    qu[1, :, NOPE_DIM:] = pltpu.roll(turned, 64, 1)[:, :ROPE_DIM].astype(jnp.bfloat16)

    for i in range(tiles):
        rows = slice(i * block, (i + 1) * block)
        n = (i + 1) * block
        parts = []
        for h in range(2):
            cols = slice(h * VALUE_DIM, (h + 1) * VALUE_DIM)
            scores = dot_nt(ku[h, :n, :], qu[h, rows, :])
            key_at = lax.broadcasted_iota(jnp.int32, (block, block), 0)
            query_at = lax.broadcasted_iota(jnp.int32, (block, block), 1)
            diag = jnp.where(key_at <= query_at, scores[n - block:], -jnp.inf)
            scores = diag if i == 0 else jnp.concatenate([scores[:n - block], diag], axis=0)
            top = jnp.max(scores, axis=0, keepdims=True)
            e = jnp.exp2((scores - top) * (scale * LOG2E))
            r = 1.0 / jnp.sum(e, axis=0, keepdims=True)
            prob_grad = dot_nt(vals[:n, cols], do_ref[rows, cols])
            center = jnp.sum(e * prob_grad, axis=0, keepdims=True) * r
            pt[h, :n, rows] = (e * r).astype(jnp.bfloat16)
            ds = (e * (r * scale) * (prob_grad - center)).astype(jnp.bfloat16)
            dst[h, :n, rows] = ds
            g = dot(kt[h, :, :n], ds)
            a = g[NOPE_DIM:NOPE_DIM + 32]
            b = g[NOPE_DIM + 32:]
            c, s = cos_t_ref[:, rows], sin_t_ref[:, rows]
            parts += [g[:NOPE_DIM], a * c + b * s, b * c - a * s]
        dq_ref[rows, :] = jnp.concatenate(parts, axis=0).T.astype(jnp.bfloat16)

    for h in range(2):
        for j in range(tiles):
            rows = slice(j * block, (j + 1) * block)
            cols = slice(h * VALUE_DIM, (h + 1) * VALUE_DIM)
            dv = dot(pt[h, rows, j * block:], do_ref[j * block:, cols])
            dk = dot(dst[h, rows, j * block:], qu[h, j * block:, :])
            dkv[rows, h * NOPE_DIM:(h + 1) * NOPE_DIM] = dk[:, :NOPE_DIM].astype(jnp.bfloat16)
            dkv[rows, (2 + h) * 128:(3 + h) * 128] = dv.astype(jnp.bfloat16)
            rot_acc[rows, :] += dk[:, NOPE_DIM:]

    dw = dot(comp_t[...], dkv[...]) * grad_scale
    dw_ref[0] = dw[:, :256].astype(dw_ref.dtype)
    dw_ref[1] = dw[:, 256:].astype(dw_ref.dtype)
    acc[...] += dot_nt(dkv[:, :256], wk_ref[...]) + dot_nt(dkv[:, 256:], wv_ref[...])

    @pl.when(step == pl.num_programs(0) - 1)
    def _():
        part_ref[...] = acc[...].astype(jnp.bfloat16)
        rot_ref[...] = rot_acc[...].astype(jnp.bfloat16)


def attention(queries, out_grad, latent, rope_key, kv_gain, key_whole, value_whole, grad_scale):
    length = queries.shape[0]
    width = latent.shape[1]
    pairs = key_whole.shape[1] // 256
    block = 256
    cosine, sine = rope_tables(length)
    cos_wide = np.tile(cosine, (1, 4))
    sin_wide = np.concatenate([-sine, sine, -sine, sine], axis=1)
    bf, f32 = jnp.bfloat16, jnp.float32
    whole = lambda shape: pl.BlockSpec(shape, lambda p: (0,) * len(shape))
    column = lambda rows, cols: pl.BlockSpec((rows, cols), lambda p: (0, p))
    return pl.pallas_call(
        functools.partial(attention_kernel, block, grad_scale),
        grid=(pairs,),
        in_specs=[
            whole((length, width)), whole((length, ROPE_DIM)), whole((1, width)),
            whole((length, 128)), whole((length, 128)),
            whole((32, length)), whole((32, length)),
            column(length, 2 * QK), column(length, 256), column(width, 256), column(width, 256),
        ],
        out_specs=[
            column(length, 2 * QK),
            pl.BlockSpec((2, width, 256), lambda p: (0, 0, p)),
            whole((length, width)), whole((length, ROPE_DIM)),
        ],
        out_shape=[
            jax.ShapeDtypeStruct(queries.shape, bf),
            jax.ShapeDtypeStruct((2, width, key_whole.shape[1]), bf),
            jax.ShapeDtypeStruct((length, width), bf),
            jax.ShapeDtypeStruct((length, ROPE_DIM), bf),
        ],
        scratch_shapes=[
            pltpu.VMEM((length, width), bf), pltpu.VMEM((width, length), bf),
            pltpu.VMEM((length, 128), bf), pltpu.VMEM((128, length), bf),
            pltpu.VMEM((2, length, QK), bf), pltpu.VMEM((2, QK, length), bf),
            pltpu.VMEM((length, 256), bf), pltpu.VMEM((2, length, QK), bf),
            pltpu.VMEM((2, length, length), bf), pltpu.VMEM((2, length, length), bf),
            pltpu.VMEM((length, 512), bf),
            pltpu.VMEM((length, width), f32), pltpu.VMEM((length, ROPE_DIM), f32),
        ],
        compiler_params=pltpu.CompilerParams(
            dimension_semantics=("arbitrary",), vmem_limit_bytes=48 * 1024 * 1024
        ),
        cost_estimate=pl.CostEstimate(flops=10_000_000_000, bytes_accessed=12_000_000, transcendentals=4_000_000),
        name="attention_backward",
    )(
        latent, rope_key, kv_gain.reshape(1, -1), cos_wide, sin_wide,
        np.ascontiguousarray(cosine.T), np.ascontiguousarray(sine.T),
        queries, out_grad, key_whole, value_whole,
    )


def finish(comp_total, rot_total, raw_latent, kv_gain, cosine, sine):
    inverse = lax.rsqrt(jnp.mean(raw_latent * raw_latent, axis=-1, keepdims=True) + norm_eps)
    mixed = comp_total * kv_gain
    spread = jnp.mean(raw_latent * mixed, axis=-1, keepdims=True)
    latent_grad = (inverse * mixed - raw_latent * inverse**3 * spread).astype(jnp.bfloat16)
    a, b = rot_total[:, :32], rot_total[:, 32:]
    rope_grad = jnp.concatenate([a * cosine + b * sine, b * cosine - a * sine], axis=-1)
    return latent_grad, rope_grad.astype(jnp.bfloat16)


def shards(queries, out_grad, latent, rope_key, kv_gain, key_up, value_up):
    ups = lax.all_gather(jnp.stack([key_up, value_up]), "dp", axis=1, tiled=True)
    length = latent.shape[1]
    grad_scale = float(lax.axis_size("dp") * length) ** (-0.5)
    query_grad, dw, part, rot = attention(
        queries[0], out_grad[0], latent[0], rope_key[0], kv_gain, ups[0], ups[1], grad_scale
    )
    dw = lax.psum_scatter(dw, "dp", scatter_dimension=1, tiled=True).astype(jnp.float32)
    comp_total = lax.psum(part, "sp").astype(jnp.float32)
    rot_total = lax.psum(rot, "sp").astype(jnp.float32)
    cosine, sine = rope_tables(length)
    latent_grad, rope_grad = finish(
        comp_total, rot_total, latent[0].astype(jnp.float32), kv_gain, cosine, sine
    )
    return query_grad[None], latent_grad[None], rope_grad[None], dw[0], dw[1]


def solution(mesh):
    return jax.shard_map(
        shards,
        mesh=mesh,
        in_specs=(
            P("dp", None, "sp"),
            P("dp", None, "sp"),
            P("dp", None, None),
            P("dp", None, None),
            P(),
            P("dp", "sp"),
            P("dp", "sp"),
        ),
        out_specs=(
            P("dp", None, "sp"),
            P("dp", None, None),
            P("dp", None, None),
            P("dp", "sp"),
            P("dp", "sp"),
        ),
        check_vma=False,
    )
```

time: 274 us -> 170 us (0.62)
  matrix products: 87 us -> 0 us
  Pallas kernels: 0 us -> 24.5 us
  local copies, waits for them, and re-layouts: 24.8 us -> 4.44 us
  other arithmetic: 22.9 us -> 5.82 us
    dot_general x45 -> x0, matrix products: 87 us -> none  [the longest x8 18.9 us: head_backward(): jnp.dot(score_grad.T, query_used, preferred_element_type=jnp.float32)]
    pallas_call x0 -> x1, Pallas kernels: none -> 24.5 us  [attention(): pl.pallas_call(functools.partial(attention_kernel, block, grad_scale), gr...]
    psum x1, waiting for transfers between devices: 32.9 us -> 47.5 us  [shards(): comp_total = lax.psum(part, 'sp').astype(jnp.float32)]
    reduce_scatter x1, waiting for transfers between devices: 50.4 us -> 41.4 us  [shards(): lax.psum_scatter(dw, 'dp', scatter_dimension=1, tiled=True)]
    unnamed x33 -> x20, local copies, waits for them, and re-layouts: 9.88 us -> 1.89 us
    all_gather x2 -> x1, waiting for transfers between devices: 36 us -> 29.1 us  [shards(): lax.all_gather(jnp.stack([key_up, value_up]), 'dp', axis=1, tiled=True)]
    dynamic_update_slice x16 -> x0, local copies, waits for them, and re-layouts: 6.73 us -> none  [attend(): lax.map(lambda items: head_backward(items[0], items[1], items[2], items[3...]
    reduce_sum x11 -> x1, other arithmetic: 6.87 us -> 0.46 us  [finish(): jnp.mean(raw_latent * raw_latent, axis=-1, keepdims=True) + norm_eps]
  transfers between devices with their start and end apart: 4 -> 3, of which waited for: 4 -> 3; matrix products, arithmetic and copies ran while one was open for 11% -> 3% of each run, Pallas kernels for 0% -> 0%
where the time goes in v1:
time: 170 us; the launch traced here: 168 us
  waiting for transfers between devices  119 us (70%)
  Pallas kernels  24.5 us (14%)
  between operations  13.9 us (8%)
  other arithmetic  5.82 us (3%)
  local copies, waits for them, and re-layouts  4.44 us (3%)
    psum x1, waiting for transfers between devices, shards(): comp_total = lax.psum(part, 'sp').astype(jnp.float32)  47.5 us
    reduce_scatter x1, waiting for transfers between devices, shards(): lax.psum_scatter(dw, 'dp', scatter_dimension=1, tiled=True)  41.4 us
    all_gather x1, waiting for transfers between devices, shards(): lax.all_gather(jnp.stack([key_up, value_up]), 'dp', axis=1, tiled=True)  29.1 us
    pallas_call x1, Pallas kernels, attention(): pl.pallas_call(functools.partial(attention_kernel, block, grad_scale), gr...  24.5 us
  transfers between devices with their start and end apart: 3, of which 3 were waited for; matrix products, arithmetic and copies ran while one was open for 3% of the time, Pallas kernels for 0%

profile of v1, /device:TPU:24, one launch (start us, length us, event | category | flops | bytes accessed | tf_op | source)
XLA Modules:
  0.0 167.5 jit_solution(7275107556441953791)
XLA Ops:
  7.2 0.0 all-gather.2.cloned.1.call-start
  7.2 1.7 %pad_maximum_fusion = bf16[2,64,1024]{2,1,0:T(8,128)(2,1)} fusion(bf16[1,64,1024]{2,1,0:T(8,128)(2,1)} %bitcast.28, bf16[1,64,1024]{2,1,0:T(8,128)(2,1)} %bitcast.29), kind=kLoop, calls=%fused_computation.16 | loop fusion | flops 131072 | bytes 524288 | tf_op jit(solution)/shard_map/stack | solution.py:201
  8.9 0.0 all-gather.2.cloned.1.call-update
  8.9 0.0 all-reduce.3.cloned.1.call-start
  9.0 1.1 copy.18
  10.0 0.0 copy-start
  10.1 0.0 copy-start.1
  10.1 0.0 copy-start.2
  10.1 0.0 copy-start.3
  10.1 0.0 copy-start.4
  10.1 0.0 copy-start.5
  10.1 29.1 %all-gather.2.cloned.1.call-done = bf16[2,512,1024]{2,1,0:T(8,128)(2,1)} async-done(((bf16[2,64,1024]{2,1,0:T(8,128)(2,1)}), bf16[2,512,1024]{2,1,0:T(8,128)(2,1)}) %all-gather.2.cloned.1.call-update) | async-done | bytes 2097168 | tf_op jit(solution)/shard_map/all_gather | solution.py:201
  39.2 1.7 %slice_bitcast_fusion = (bf16[512,1024]{1,0:T(8,128)(2,1)S(1)}, bf16[512,1024]{1,0:T(8,128)(2,1)S(1)}) fusion(bf16[2,512,1024]{2,1,0:T(8,128)(2,1)} %all-gather.2.cloned.1.call-done), kind=kLoop, calls=%fused_computation.9 | loop fusion | bytes 4194304 | tf_op jit(solution)/shard_map/squeeze | solution.py:205
  41.0 0.0 copy-done
  41.0 0.0 copy-done.1
  41.0 0.0 copy-done.2
  41.0 0.0 copy-done.3
  41.0 0.0 copy-done.4
  41.0 0.0 copy-done.5
  41.0 24.5 %attention_backward.1 = (bf16[768,1536]{1,0:T(8,128)(2,1)}, bf16[2,512,1024]{2,1,0:T(8,128)(2,1)}, bf16[768,512]{1,0:T(8,128)(2,1)}, bf16[768,64]{1,0:T(8,128)(2,1)}) custom-call(bf16[768,512]{1,0:T(8,128)(2,1)S(1)} %bitcast.25, bf16[768,64]{1,0:T(8,128)(2,1)S(1)} %bitcast.26, f32[1,512]{1,0:T(1,128)S(1)} %bitcast.27, f32[768,128]{1,0:T(8,128)S(1)} %copy-done.3, ...), custom_call_target="tpu_custom_call" | custom-call | flops 10000000000 | bytes 12000000 | tf_op jit(solution)/shard_map/attention_backward/pallas_call | solution.py:149
  65.5 0.0 all-reduce.3.cloned.1.call-update
  65.5 0.0 copy-start.7
  65.5 0.0 copy-start.8
  65.5 0.0 reduce-scatter.2.cloned.1.call-start
  65.6 0.7 reduce-scatter.2.cloned.1.call-update
  66.3 47.5 %all-reduce.3.cloned.1.call-done = (bf16[768,512]{1,0:T(8,128)(2,1)}, bf16[768,64]{1,0:T(8,128)(2,1)}) async-done(((bf16[768,512]{1,0:T(8,128)(2,1)}, bf16[768,64]{1,0:T(8,128)(2,1)}), (bf16[768,512]{1,0:T(8,128)(2,1)}, bf16[768,64]{1,0:T(8,128)(2,1)})) %all-reduce.3.cloned.1.call-update) | async-done | bytes 884752 | tf_op jit(solution)/shard_map/psum | solution.py:208
  113.8 1.0 convert_element_type.26
  114.8 0.0 copy-done.7
  114.8 0.0 copy-done.8
  114.8 0.0 copy-start.6
  114.8 0.2 fusion.6
  115.0 0.1 pad_maximum_fusion.1
  115.2 0.8 copy.19
  115.9 0.0 copy-done.6
  115.9 0.5 fusion
  116.4 1.3 fusion.5
  117.8 41.4 %reduce-scatter.2.cloned.1.call-done = bf16[2,64,1024]{2,1,0:T(8,128)(2,1)} async-done(((bf16[2,512,1024]{2,1,0:T(8,128)(2,1)}), bf16[2,64,1024]{2,1,0:T(8,128)(2,1)}) %reduce-scatter.2.cloned.1.call-update) | async-done | bytes 262160 | tf_op jit(solution)/shard_map/reduce_scatter | solution.py:207
  159.1 1.0 convert_element_type.27
  160.1 0.8 slice_bitcast_fusion.2
  (2 shorter events, 0.0 us)
Async XLA Ops:
  7.2 32.1 %all-gather.2.cloned.1.call-start = ((), (), s32[]{:S(2)}) async-start(), calls=%async_computation.1 | async-start | bytes 2359296 | tf_op jit(solution)/shard_map/all_gather | solution.py:201
  8.9 104.9 %all-reduce.3.cloned.1.call-start = ((), (), s32[]{:S(2)}) async-start(), calls=%async_computation.3 | async-start | bytes 1966080 | tf_op jit(solution)/shard_map/psum | solution.py:208
  10.0 30.9 %copy-start = (bf16[1,768,512]{2,1,0:T(8,128)(2,1)S(1)}, bf16[1,768,512]{2,1,0:T(8,128)(2,1)}, u32[]{:S(2)}) copy-start(bf16[1,768,512]{2,1,0:T(8,128)(2,1)} %param.15) | copy-start | bytes 2359300
  10.1 30.9 %copy-start.1 = (f32[512]{0:T(512)S(1)}, f32[512]{0:T(512)}, u32[]{:S(2)}) copy-start(f32[512]{0:T(512)} %param.17) | copy-start | bytes 6148
  10.1 30.9 %copy-start.2 = (f32[768,128]{1,0:T(8,128)S(1)}, f32[768,128]{1,0:T(8,128)}, u32[]{:S(2)}) copy-start(f32[768,128]{1,0:T(8,128)} %constant.21.clone.sin_ref) | copy-start | bytes 1179652
  10.1 30.9 %copy-start.3 = (f32[768,128]{1,0:T(8,128)S(1)}, f32[768,128]{1,0:T(8,128)}, u32[]{:S(2)}) copy-start(f32[768,128]{1,0:T(8,128)} %constant.20.clone.cos_ref) | copy-start | bytes 1179652
  10.1 30.9 %copy-start.4 = (f32[32,768]{1,0:T(8,128)S(1)}, f32[32,768]{1,0:T(8,128)}, u32[]{:S(2)}) copy-start(f32[32,768]{1,0:T(8,128)} %constant.23.clone.sin_t_ref) | copy-start | bytes 294916
  10.1 30.9 %copy-start.5 = (f32[32,768]{1,0:T(8,128)S(1)}, f32[32,768]{1,0:T(8,128)}, u32[]{:S(2)}) copy-start(f32[32,768]{1,0:T(8,128)} %constant.22.clone.cos_t_ref) | copy-start | bytes 294916
  65.5 49.3 %copy-start.7 = (f32[768,32]{1,0:T(8,128)S(1)}, f32[768,32]{1,0:T(8,128)}, u32[]{:S(2)}) copy-start(f32[768,32]{1,0:T(8,128)} %constant.25.clone) | copy-start | bytes 294916
  65.5 49.3 %copy-start.8 = (f32[768,32]{1,0:T(8,128)S(1)}, f32[768,32]{1,0:T(8,128)}, u32[]{:S(2)}) copy-start(f32[768,32]{1,0:T(8,128)} %constant.24.clone) | copy-start | bytes 294916
  65.5 93.6 %reduce-scatter.2.cloned.1.call-start = ((), (), s32[]{:S(2)}) async-start(), calls=%async_computation.2 | async-start | bytes 2359296 | tf_op jit(solution)/shard_map/reduce_scatter | solution.py:207
  114.8 1.2 copy-start.6
Sparse Core Ops, SparseCore 0:
  10.4 28.7 all-gather.1
  65.6 48.1 all-reduce.2
  117.1 42.0 reduce-scatter.1

commit v2 on v1

--- a/solution.py
+++ b/solution.py
@@ -44,7 +44,7 @@
     block, grad_scale,
     latent_ref, rope_ref, gain_ref, cos_ref, sin_ref, cos_t_ref, sin_t_ref,
     q_ref, do_ref, wk_ref, wv_ref,
-    dq_ref, dw_ref, part_ref, rot_ref,
+    dq_ref, dw_ref, part_ref,
     comp, comp_t, krot, krot_t, ku, kt, vals, qu, pt, dst, dkv, acc, rot_acc,
 ):
     step = pl.program_id(0)
@@ -125,17 +125,19 @@
             rot_acc[rows, :] += dk[:, NOPE_DIM:]
 
     dw = dot(comp_t[...], dkv[...]) * grad_scale
-    dw_ref[0] = dw[:, :256].astype(dw_ref.dtype)
-    dw_ref[1] = dw[:, 256:].astype(dw_ref.dtype)
+    dw_ref[:, 0] = dw[:, :256].reshape(dw_ref.shape[0], dw_ref.shape[2], 256).astype(dw_ref.dtype)
+    dw_ref[:, 1] = dw[:, 256:].reshape(dw_ref.shape[0], dw_ref.shape[2], 256).astype(dw_ref.dtype)
     acc[...] += dot_nt(dkv[:, :256], wk_ref[...]) + dot_nt(dkv[:, 256:], wv_ref[...])
 
     @pl.when(step == pl.num_programs(0) - 1)
     def _():
-        part_ref[...] = acc[...].astype(jnp.bfloat16)
-        rot_ref[...] = rot_acc[...].astype(jnp.bfloat16)
-
-
-def attention(queries, out_grad, latent, rope_key, kv_gain, key_whole, value_whole, grad_scale):
+        width = acc.shape[1]
+        rot = rot_acc[...].astype(jnp.bfloat16)
+        part_ref[:, :width] = acc[...].astype(jnp.bfloat16)
+        part_ref[:, width:] = jnp.concatenate([rot, rot], axis=1)
+
+
+def attention(queries, out_grad, latent, rope_key, kv_gain, key_whole, value_whole, grad_scale, n_dp):
     length = queries.shape[0]
     width = latent.shape[1]
     pairs = key_whole.shape[1] // 256
@@ -157,14 +159,13 @@
         ],
         out_specs=[
             column(length, 2 * QK),
-            pl.BlockSpec((2, width, 256), lambda p: (0, 0, p)),
-            whole((length, width)), whole((length, ROPE_DIM)),
+            pl.BlockSpec((n_dp, 2, width // n_dp, 256), lambda p: (0, 0, 0, p)),
+            whole((length, width + 128)),
         ],
         out_shape=[
             jax.ShapeDtypeStruct(queries.shape, bf),
-            jax.ShapeDtypeStruct((2, width, key_whole.shape[1]), bf),
-            jax.ShapeDtypeStruct((length, width), bf),
-            jax.ShapeDtypeStruct((length, ROPE_DIM), bf),
+            jax.ShapeDtypeStruct((n_dp, 2, width // n_dp, key_whole.shape[1]), bf),
+            jax.ShapeDtypeStruct((length, width + 128), bf),
         ],
         scratch_shapes=[
             pltpu.VMEM((length, width), bf), pltpu.VMEM((width, length), bf),
@@ -187,31 +188,118 @@
     )
 
 
-def finish(comp_total, rot_total, raw_latent, kv_gain, cosine, sine):
-    inverse = lax.rsqrt(jnp.mean(raw_latent * raw_latent, axis=-1, keepdims=True) + norm_eps)
-    mixed = comp_total * kv_gain
-    spread = jnp.mean(raw_latent * mixed, axis=-1, keepdims=True)
-    latent_grad = (inverse * mixed - raw_latent * inverse**3 * spread).astype(jnp.bfloat16)
-    a, b = rot_total[:, :32], rot_total[:, 32:]
-    rope_grad = jnp.concatenate([a * cosine + b * sine, b * cosine - a * sine], axis=-1)
-    return latent_grad, rope_grad.astype(jnp.bfloat16)
+def exchange_kernel(
+    n_sp, n_dp,
+    dw_ref, part_ref, latent_ref, gain_ref, cos_ref, sin_ref,
+    grad_ref, low_ref,
+    got_part, got_dw, send_a, recv_a, send_b, recv_b, send_c, recv_c,
+):
+    sp, dp = lax.axis_index("sp"), lax.axis_index("dp")
+    rows = latent_ref.shape[0] // n_sp
+    width = latent_ref.shape[1]
+    mine = pl.ds(pl.multiple_of(sp * rows, rows), rows)
+    mesh_id = pl.DeviceIdType.MESH
+    barrier = pltpu.get_barrier_semaphore()
+
+    def each(count, act):
+        def body(k, carry):
+            act(k)
+            return carry
+        lax.fori_loop(1, count, body, 0)
+
+    def greet(axis, here, count):
+        each(count, lambda k: pl.semaphore_signal(
+            barrier, inc=1, device_id={axis: lax.rem(here + k, count)}, device_id_type=mesh_id))
+
+    greet("sp", sp, n_sp)
+    greet("dp", dp, n_dp)
+    pl.semaphore_wait(barrier, n_sp + n_dp - 2)
+
+    def part_copy(k):
+        peer = lax.rem(sp + k, n_sp)
+        return pltpu.make_async_remote_copy(
+            src_ref=part_ref.at[pl.ds(pl.multiple_of(peer * rows, rows), rows)],
+            dst_ref=got_part.at[k], send_sem=send_a.at[k], recv_sem=recv_a.at[k],
+            device_id={"sp": peer}, device_id_type=mesh_id)
+
+    def dw_copy(k):
+        peer = lax.rem(dp + k, n_dp)
+        return pltpu.make_async_remote_copy(
+            src_ref=dw_ref.at[peer], dst_ref=got_dw.at[k],
+            send_sem=send_b.at[k], recv_sem=recv_b.at[k],
+            device_id={"dp": peer}, device_id_type=mesh_id)
+
+    def low_copy(k):
+        return pltpu.make_async_remote_copy(
+            src_ref=low_ref.at[mine], dst_ref=low_ref.at[mine],
+            send_sem=send_c.at[k], recv_sem=recv_c.at[k],
+            device_id={"sp": lax.rem(sp + k, n_sp)}, device_id_type=mesh_id)
+
+    each(n_sp, lambda k: part_copy(k).start())
+    each(n_dp, lambda k: dw_copy(k).start())
+
+    total = part_ref[mine, :].astype(jnp.float32)
+    each(n_sp, lambda k: part_copy(k).wait())
+    for k in range(1, n_sp):
+        total = total + got_part[k].astype(jnp.float32)
+    raw = latent_ref[mine, :].astype(jnp.float32)
+    inverse = lax.rsqrt(jnp.mean(raw * raw, axis=-1, keepdims=True) + norm_eps)
+    mixed = total[:, :width] * gain_ref[...]
+    spread = jnp.mean(raw * mixed, axis=-1, keepdims=True)
+    low_ref[mine, :width] = (inverse * mixed - raw * inverse**3 * spread).astype(jnp.bfloat16)
+    rot = total[:, width:]
+    low_ref[mine, width:] = (
+        rot * cos_ref[mine, :] - swap_halves(rot) * sin_ref[mine, :]
+    ).astype(jnp.bfloat16)
+    each(n_sp, lambda k: low_copy(k).start())
+
+    grad_ref[...] = dw_ref[dp].astype(jnp.float32)
+    def add(k):
+        dw_copy(k).wait()
+        grad_ref[...] += got_dw[k].astype(jnp.float32)
+    each(n_dp, add)
+    each(n_sp, lambda k: low_copy(k).wait())
+
+
+def exchange(dw, part, latent, kv_gain, n_sp, n_dp):
+    length, width = latent.shape
+    cosine, sine = rope_tables(length)
+    bf = jnp.bfloat16
+    vmem = pl.BlockSpec(memory_space=pltpu.VMEM)
+    sems = lambda n: pltpu.SemaphoreType.DMA((n,))
+    return pl.pallas_call(
+        functools.partial(exchange_kernel, n_sp, n_dp),
+        in_specs=[vmem] * 6,
+        out_specs=[vmem] * 2,
+        out_shape=[
+            jax.ShapeDtypeStruct(dw.shape[1:], jnp.float32),
+            jax.ShapeDtypeStruct(part.shape, bf),
+        ],
+        scratch_shapes=[
+            pltpu.VMEM((n_sp, length // n_sp, part.shape[1]), bf),
+            pltpu.VMEM(dw.shape, bf),
+            sems(n_sp), sems(n_sp), sems(n_dp), sems(n_dp), sems(n_sp), sems(n_sp),
+        ],
+        compiler_params=pltpu.CompilerParams(
+            collective_id=0, has_side_effects=True, vmem_limit_bytes=32 * 1024 * 1024
+        ),
+        name="exchange",
+    )(
+        dw, part, latent, kv_gain.reshape(1, -1), np.tile(cosine, (1, 4)),
+        np.concatenate([-sine, sine, -sine, sine], axis=1),
+    )
 
 
 def shards(queries, out_grad, latent, rope_key, kv_gain, key_up, value_up):
     ups = lax.all_gather(jnp.stack([key_up, value_up]), "dp", axis=1, tiled=True)
-    length = latent.shape[1]
-    grad_scale = float(lax.axis_size("dp") * length) ** (-0.5)
-    query_grad, dw, part, rot = attention(
-        queries[0], out_grad[0], latent[0], rope_key[0], kv_gain, ups[0], ups[1], grad_scale
+    length, width = latent.shape[1:]
+    n_sp, n_dp = lax.axis_size("sp"), lax.axis_size("dp")
+    grad_scale = float(n_dp * length) ** (-0.5)
+    query_grad, dw, part = attention(
+        queries[0], out_grad[0], latent[0], rope_key[0], kv_gain, ups[0], ups[1], grad_scale, n_dp
     )
-    dw = lax.psum_scatter(dw, "dp", scatter_dimension=1, tiled=True).astype(jnp.float32)
-    comp_total = lax.psum(part, "sp").astype(jnp.float32)
-    rot_total = lax.psum(rot, "sp").astype(jnp.float32)
-    cosine, sine = rope_tables(length)
-    latent_grad, rope_grad = finish(
-        comp_total, rot_total, latent[0].astype(jnp.float32), kv_gain, cosine, sine
-    )
-    return query_grad[None], latent_grad[None], rope_grad[None], dw[0], dw[1]
+    dw, low = exchange(dw, part, latent[0], kv_gain, n_sp, n_dp)
+    return query_grad[None], low[None, :, :width], low[None, :, width:width + ROPE_DIM], dw[0], dw[1]
 
 
 def solution(mesh):

time: 170 us -> 123 us (0.72); the launches traced: 168 us -> 123 us
  waiting for transfers between devices: 119 us -> 29.2 us
  Pallas kernels: 24.5 us -> 71.2 us
  other arithmetic: 5.82 us -> 1.7 us
  local copies, waits for them, and re-layouts: 4.44 us -> 6.97 us
    psum x1 -> x0, waiting for transfers between devices: 47.5 us -> none  [shards(): comp_total = lax.psum(part, 'sp').astype(jnp.float32)]
    pallas_call x0 -> x1, Pallas kernels: none -> 47.1 us  [exchange(): pl.pallas_call(functools.partial(exchange_kernel, n_sp, n_dp), in_specs=[...]
    reduce_scatter x1 -> x0, waiting for transfers between devices: 41.4 us -> none  [shards(): lax.psum_scatter(dw, 'dp', scatter_dimension=1, tiled=True)]
    convert_element_type x2 -> x0, other arithmetic: 1.94 us -> none  [the longest x1 0.99 us: shards(): lax.psum_scatter(dw, 'dp', scatter_dimension=1, tiled=True)]
    unnamed x20 -> x16, local copies, waits for them, and re-layouts: 1.89 us -> 3.47 us
  transfers between devices with their start and end apart: 3 -> 1, of which waited for: 3 -> 1; matrix products, arithmetic and copies ran while one was open for 3% -> 1% of each run, Pallas kernels for 0% -> 0%
where the time goes in v2:
time: 123 us
  Pallas kernels  71.2 us (58%)
  waiting for transfers between devices  29.2 us (24%)
  between operations  14.2 us (12%)
  local copies, waits for them, and re-layouts  6.97 us (6%)
  other arithmetic  1.7 us (1%)
    pallas_call x1, Pallas kernels, exchange(): pl.pallas_call(functools.partial(exchange_kernel, n_sp, n_dp), in_specs=[...  47.1 us
    all_gather x1, waiting for transfers between devices, shards(): lax.all_gather(jnp.stack([key_up, value_up]), 'dp', axis=1, tiled=True)  29.2 us
    pallas_call x1, Pallas kernels, attention(): pl.pallas_call(functools.partial(attention_kernel, block, grad_scale), gr...  24.1 us
    unnamed x16, local copies, waits for them, and re-layouts  3.47 us
  transfers between devices with their start and end apart: 1, of which 1 were waited for; matrix products, arithmetic and copies ran while one was open for 1% of the time, Pallas kernels for 0%

profile of v2, /device:TPU:24, one launch (start us, length us, event | category | flops | bytes accessed | tf_op | source)
XLA Modules:
  0.0 123.2 jit_solution(15051106676165919542)
XLA Ops:
  7.2 0.0 all-gather.2.cloned.1.call-start
  7.2 1.7 %pad_maximum_fusion = bf16[2,64,1024]{2,1,0:T(8,128)(2,1)} fusion(bf16[1,64,1024]{2,1,0:T(8,128)(2,1)} %bitcast.25, bf16[1,64,1024]{2,1,0:T(8,128)(2,1)} %bitcast.26), kind=kLoop, calls=%fused_computation.3 | loop fusion | flops 131072 | bytes 524288 | tf_op jit(solution)/shard_map/stack | solution.py:294
  8.9 0.0 all-gather.2.cloned.1.call-update
  8.9 1.1 copy.18
  10.0 0.0 copy-start.1
  10.0 0.0 copy-start.2
  10.0 0.0 copy-start.3
  10.0 0.0 copy-start.4
  10.1 0.0 copy-start.5
  10.1 0.0 copy-start.6
  10.1 29.2 %all-gather.2.cloned.1.call-done = bf16[2,512,1024]{2,1,0:T(8,128)(2,1)} async-done(((bf16[2,64,1024]{2,1,0:T(8,128)(2,1)}), bf16[2,512,1024]{2,1,0:T(8,128)(2,1)}) %all-gather.2.cloned.1.call-update) | async-done | bytes 2097168 | tf_op jit(solution)/shard_map/all_gather | solution.py:294
  39.2 1.7 %slice_bitcast_fusion = (bf16[512,1024]{1,0:T(8,128)(2,1)S(1)}, bf16[512,1024]{1,0:T(8,128)(2,1)S(1)}) fusion(bf16[2,512,1024]{2,1,0:T(8,128)(2,1)} %all-gather.2.cloned.1.call-done), kind=kLoop, calls=%fused_computation | loop fusion | bytes 4194304 | tf_op jit(solution)/shard_map/squeeze | solution.py:299
  41.0 0.0 copy-done.1
  41.0 0.0 copy-done.2
  41.0 0.0 copy-done.3
  41.0 0.0 copy-done.4
  41.0 0.0 copy-done.5
  41.0 0.0 copy-done.6
  41.0 24.1 %attention_backward.1 = (bf16[768,1536]{1,0:T(8,128)(2,1)}, bf16[8,2,64,1024]{3,2,1,0:T(8,128)(2,1)}, bf16[768,640]{1,0:T(8,128)(2,1)S(1)}) custom-call(bf16[768,512]{1,0:T(8,128)(2,1)S(1)} %bitcast.20, bf16[768,64]{1,0:T(8,128)(2,1)S(1)} %bitcast.22, f32[1,512]{1,0:T(1,128)S(1)} %bitcast.23, f32[768,128]{1,0:T(8,128)S(1)} %copy-done.3, ...), custom_call_target="tpu_custom_call" | custom-call | flops 10000000000 | bytes 12000000 | tf_op jit(solution)/shard_map/attention_backward/pallas_call | solution.py:151
  65.1 0.0 copy-start
  65.1 1.6 %copy-done = bf16[8,2,64,1024]{3,2,1,0:T(8,128)(2,1)S(1)} copy-done((bf16[8,2,64,1024]{3,2,1,0:T(8,128)(2,1)S(1)}, bf16[8,2,64,1024]{3,2,1,0:T(8,128)(2,1)}, u32[]{:S(2)}) %copy-start) | copy-done | bytes 2097176
  66.7 47.1 %exchange.1 = (f32[2,64,1024]{2,1,0:T(8,128)S(1)}, bf16[768,640]{1,0:T(8,128)(2,1)S(1)}) custom-call(bf16[8,2,64,1024]{3,2,1,0:T(8,128)(2,1)S(1)} %copy-done, bf16[768,640]{1,0:T(8,128)(2,1)S(1)} %get-tuple-element.12.part_ref, bf16[768,512]{1,0:T(8,128)(2,1)S(1)} %bitcast.21, f32[1,512]{1,0:T(1,128)S(1)} %bitcast.24, f32[768,128]{1,0:T(8,128)S(1)} %copy-done.3, ...), custom_call_target="tpu_custom_call" | custom-call | tf_op jit(solution)/shard_map/exchange/pallas_call | solution.py:270
  113.8 0.9 slice_bitcast_fusion.2
  114.8 0.8 slice_bitcast_fusion.3
  115.6 0.8 copy.19
  (1 shorter events, 0.0 us)
Async XLA Ops:
  7.2 32.1 %all-gather.2.cloned.1.call-start = ((), (), s32[]{:S(2)}) async-start(), calls=%async_computation | async-start | bytes 2359296 | tf_op jit(solution)/shard_map/all_gather | solution.py:294
  10.0 30.9 %copy-start.1 = (bf16[1,768,512]{2,1,0:T(8,128)(2,1)S(1)}, bf16[1,768,512]{2,1,0:T(8,128)(2,1)}, u32[]{:S(2)}) copy-start(bf16[1,768,512]{2,1,0:T(8,128)(2,1)} %param.15) | copy-start | bytes 2359300
  10.0 30.9 %copy-start.2 = (f32[768,128]{1,0:T(8,128)S(1)}, f32[768,128]{1,0:T(8,128)}, u32[]{:S(2)}) copy-start(f32[768,128]{1,0:T(8,128)} %constant.9.clone.sin_ref) | copy-start | bytes 1179652
  10.0 30.9 %copy-start.3 = (f32[768,128]{1,0:T(8,128)S(1)}, f32[768,128]{1,0:T(8,128)}, u32[]{:S(2)}) copy-start(f32[768,128]{1,0:T(8,128)} %constant.8.clone.cos_ref) | copy-start | bytes 1179652
  10.0 30.9 %copy-start.4 = (f32[512]{0:T(512)S(1)}, f32[512]{0:T(512)}, u32[]{:S(2)}) copy-start(f32[512]{0:T(512)} %param.17) | copy-start | bytes 6148
  10.1 30.9 %copy-start.5 = (f32[32,768]{1,0:T(8,128)S(1)}, f32[32,768]{1,0:T(8,128)}, u32[]{:S(2)}) copy-start(f32[32,768]{1,0:T(8,128)} %constant.11.clone.sin_t_ref) | copy-start | bytes 294916
  10.1 30.9 %copy-start.6 = (f32[32,768]{1,0:T(8,128)S(1)}, f32[32,768]{1,0:T(8,128)}, u32[]{:S(2)}) copy-start(f32[32,768]{1,0:T(8,128)} %constant.10.clone.cos_t_ref) | copy-start | bytes 294916
  65.1 1.6 %copy-start = (bf16[8,2,64,1024]{3,2,1,0:T(8,128)(2,1)S(1)}, bf16[8,2,64,1024]{3,2,1,0:T(8,128)(2,1)}, u32[]{:S(2)}) copy-start(bf16[8,2,64,1024]{3,2,1,0:T(8,128)(2,1)} %get-tuple-element.11.dw_ref) | copy-start | bytes 6291460
Sparse Core Ops, SparseCore 0:
  10.4 28.7 all-gather.1

commit v3 on v2

--- a/solution.py
+++ b/solution.py
@@ -290,13 +290,94 @@
     )
 
 
+def gather_kernel(
+    n_dp, key_ref, value_ref, key_out, value_out, send_a, recv_a, send_b, recv_b
+):
+    dp = lax.axis_index("dp")
+    chips = n_dp // 2
+    chip, core = dp // 2, lax.rem(dp, 2)
+    partner = chip * 2 + 1 - core
+    mesh_id = pl.DeviceIdType.MESH
+    barrier = pltpu.get_barrier_semaphore()
+    pairs = ((key_ref, key_out), (value_ref, value_out))
+
+    def each(act):
+        def body(k, carry):
+            act(k)
+            return carry
+        lax.fori_loop(1, chips, body, 0)
+
+    def other(k):
+        return lax.rem(chip + k, chips) * 2 + core
+
+    def source(k):
+        return lax.rem(chip - k + chips, chips) * 2 + core
+
+    each(lambda k: pl.semaphore_signal(
+        barrier, inc=1, device_id={"dp": other(k)}, device_id_type=mesh_id))
+    pl.semaphore_signal(barrier, inc=1, device_id={"dp": partner}, device_id_type=mesh_id)
+    pl.semaphore_wait(barrier, chips)
+
+    def far(t, k):
+        return pltpu.make_async_remote_copy(
+            src_ref=pairs[t][0], dst_ref=pairs[t][1].at[dp],
+            send_sem=send_a.at[t, k], recv_sem=recv_a.at[t, k],
+            device_id={"dp": other(k)}, device_id_type=mesh_id)
+
+    def near(t, k, own):
+        block = dp if own else source(k)
+        return pltpu.make_async_remote_copy(
+            src_ref=pairs[t][0] if own else pairs[t][1].at[block],
+            dst_ref=pairs[t][1].at[block],
+            send_sem=send_b.at[t, k], recv_sem=recv_b.at[t, k],
+            device_id={"dp": partner}, device_id_type=mesh_id)
+
+    for t in range(2):
+        each(lambda k: far(t, k).start())
+    for t in range(2):
+        near(t, 0, True).start()
+        pairs[t][1][dp] = pairs[t][0][...]
+
+    def forward(k):
+        for t in range(2):
+            far(t, k).wait_recv()
+            near(t, k, False).start()
+
+    def drain(k):
+        for t in range(2):
+            far(t, k).wait_send()
+            near(t, k, False).wait()
+
+    each(forward)
+    for t in range(2):
+        near(t, 0, True).wait()
+    each(drain)
+
+
+def gather(key_up, value_up, n_dp):
+    vmem = pl.BlockSpec(memory_space=pltpu.VMEM)
+    shape = jax.ShapeDtypeStruct((n_dp, *key_up.shape), key_up.dtype)
+    outs = pl.pallas_call(
+        functools.partial(gather_kernel, n_dp),
+        in_specs=[vmem] * 2,
+        out_specs=[vmem] * 2,
+        out_shape=[shape, shape],
+        scratch_shapes=[pltpu.SemaphoreType.DMA((2, n_dp // 2))] * 4,
+        compiler_params=pltpu.CompilerParams(
+            collective_id=1, has_side_effects=True, vmem_limit_bytes=16 * 1024 * 1024
+        ),
+        name="gather",
+    )(key_up, value_up)
+    return [out.reshape(n_dp * key_up.shape[0], -1) for out in outs]
+
+
 def shards(queries, out_grad, latent, rope_key, kv_gain, key_up, value_up):
-    ups = lax.all_gather(jnp.stack([key_up, value_up]), "dp", axis=1, tiled=True)
     length, width = latent.shape[1:]
     n_sp, n_dp = lax.axis_size("sp"), lax.axis_size("dp")
     grad_scale = float(n_dp * length) ** (-0.5)
+    key_whole, value_whole = gather(key_up, value_up, n_dp)
     query_grad, dw, part = attention(
-        queries[0], out_grad[0], latent[0], rope_key[0], kv_gain, ups[0], ups[1], grad_scale, n_dp
+        queries[0], out_grad[0], latent[0], rope_key[0], kv_gain, key_whole, value_whole, grad_scale, n_dp
     )
     dw, low = exchange(dw, part, latent[0], kv_gain, n_sp, n_dp)
     return query_grad[None], low[None, :, :width], low[None, :, width:width + ROPE_DIM], dw[0], dw[1]

time: 123 us -> 102 us (0.83)
  waiting for transfers between devices: 29.2 us -> 0 us
  Pallas kernels: 71.2 us -> 88 us
  between operations: 14.2 us -> 0.68 us
  local copies, waits for them, and re-layouts: 6.97 us -> 12.6 us
  other arithmetic: 1.7 us -> 0 us
    all_gather x1 -> x0, waiting for transfers between devices: 29.2 us -> none  [shards(): lax.all_gather(jnp.stack([key_up, value_up]), 'dp', axis=1, tiled=True)]
    pallas_call x0 -> x1, Pallas kernels: none -> 16.3 us  [gather(): pl.pallas_call(functools.partial(gather_kernel, n_dp), in_specs=[vmem] *...]
    unnamed x16 -> x20, local copies, waits for them, and re-layouts: 3.47 us -> 10.8 us
    squeeze x1 -> x0, local copies, waits for them, and re-layouts: 1.71 us -> none  [shards(): ups[1]]
    another operation x1 -> x0, other arithmetic: 1.7 us -> none  [shards(): jnp.stack([key_up, value_up])]
  transfers between devices with their start and end apart: 1 -> 0, of which waited for: 1 -> 0; matrix products, arithmetic and copies ran while one was open for 1% -> 0% of each run, Pallas kernels for 0% -> 0%
where the time goes in v3:
time: 102 us; the launch traced here: 101 us
  Pallas kernels  88 us (86%)
  local copies, waits for them, and re-layouts  12.6 us (12%)
    pallas_call x1, Pallas kernels, exchange(): pl.pallas_call(functools.partial(exchange_kernel, n_sp, n_dp), in_specs=[...  47.6 us
    pallas_call x1, Pallas kernels, attention(): pl.pallas_call(functools.partial(attention_kernel, block, grad_scale), gr...  24.1 us
    pallas_call x1, Pallas kernels, gather(): pl.pallas_call(functools.partial(gather_kernel, n_dp), in_specs=[vmem] *...  16.3 us
    unnamed x20, local copies, waits for them, and re-layouts  10.8 us

profile of v3, /device:TPU:24, one launch (start us, length us, event | category | flops | bytes accessed | tf_op | source)
XLA Modules:
  0.0 101.3 jit_solution(16819541679079853783)
XLA Ops:
  0.6 1.1 %copy.18 = bf16[1,768,64]{2,1,0:T(8,128)(2,1)S(1)} copy(bf16[1,768,64]{1,2,0:T(8,128)(2,1)} %param.16) | data formatting | bytes 196608 | tf_op args[3]
  1.7 0.0 copy-start.4
  1.7 0.9 copy-done.4
  2.6 0.0 copy-start.5
  2.6 0.9 copy-done.5
  3.5 16.3 %gather.1 = (bf16[8,64,1024]{2,1,0:T(8,128)(2,1)S(1)}, bf16[8,64,1024]{2,1,0:T(8,128)(2,1)S(1)}) custom-call(bf16[64,1024]{1,0:T(8,128)(2,1)S(1)} %copy-done.4, bf16[64,1024]{1,0:T(8,128)(2,1)S(1)} %copy-done.5), custom_call_target="tpu_custom_call" | custom-call | tf_op jit(solution)/shard_map/gather/pallas_call | solution.py:360
  19.8 0.0 copy-start.1
  19.8 1.1 %copy-done.1 = bf16[1,768,512]{2,1,0:T(8,128)(2,1)S(1)} copy-done((bf16[1,768,512]{2,1,0:T(8,128)(2,1)S(1)}, bf16[1,768,512]{2,1,0:T(8,128)(2,1)}, u32[]{:S(2)}) %copy-start.1) | copy-done | bytes 786456
  20.9 0.0 copy-start.2
  20.9 1.0 copy-done.2
  21.9 0.0 copy-start.3
  21.9 1.0 copy-done.3
  22.9 0.0 copy-start.6
  22.9 0.7 copy-done.6
  23.6 0.0 copy-start.7
  23.6 0.9 copy-done.7
  24.5 0.0 copy-start.8
  24.5 0.9 copy-done.8
  25.4 24.1 %attention_backward.1 = (bf16[768,1536]{1,0:T(8,128)(2,1)}, bf16[8,2,64,1024]{3,2,1,0:T(8,128)(2,1)}, bf16[768,640]{1,0:T(8,128)(2,1)S(1)}) custom-call(bf16[768,512]{1,0:T(8,128)(2,1)S(1)} %bitcast.16, bf16[768,64]{1,0:T(8,128)(2,1)S(1)} %bitcast.18, f32[1,512]{1,0:T(1,128)S(1)} %bitcast.19, f32[768,128]{1,0:T(8,128)S(1)} %copy-done.3, ...), custom_call_target="tpu_custom_call" | custom-call | flops 10000000000 | bytes 12000000 | tf_op jit(solution)/shard_map/attention_backward/pallas_call | solution.py:151
  49.5 0.0 copy-start
  49.5 1.6 %copy-done = bf16[8,2,64,1024]{3,2,1,0:T(8,128)(2,1)S(1)} copy-done((bf16[8,2,64,1024]{3,2,1,0:T(8,128)(2,1)S(1)}, bf16[8,2,64,1024]{3,2,1,0:T(8,128)(2,1)}, u32[]{:S(2)}) %copy-start) | copy-done | bytes 2097176
  51.1 47.6 %exchange.1 = (f32[2,64,1024]{2,1,0:T(8,128)S(1)}, bf16[768,640]{1,0:T(8,128)(2,1)S(1)}) custom-call(bf16[8,2,64,1024]{3,2,1,0:T(8,128)(2,1)S(1)} %copy-done, bf16[768,640]{1,0:T(8,128)(2,1)S(1)} %get-tuple-element.16.part_ref, bf16[768,512]{1,0:T(8,128)(2,1)S(1)} %bitcast.17, f32[1,512]{1,0:T(1,128)S(1)} %bitcast.20, f32[768,128]{1,0:T(8,128)S(1)} %copy-done.3, ...), custom_call_target="tpu_custom_call" | custom-call | tf_op jit(solution)/shard_map/exchange/pallas_call | solution.py:270
  98.8 0.8 slice_bitcast_fusion.1
  99.6 0.9 slice_bitcast_fusion
  100.6 0.8 copy.19
  (1 shorter events, 0.0 us)
Async XLA Ops:
  1.7 0.9 copy-start.4
  2.6 0.9 copy-start.5
  19.8 1.1 %copy-start.1 = (bf16[1,768,512]{2,1,0:T(8,128)(2,1)S(1)}, bf16[1,768,512]{2,1,0:T(8,128)(2,1)}, u32[]{:S(2)}) copy-start(bf16[1,768,512]{2,1,0:T(8,128)(2,1)} %param.15) | copy-start | bytes 2359300
  20.9 1.0 copy-start.2
  21.9 1.0 copy-start.3
  22.9 0.7 copy-start.6
  23.6 0.9 copy-start.7
  24.5 0.9 copy-start.8
  49.5 1.6 %copy-start = (bf16[8,2,64,1024]{3,2,1,0:T(8,128)(2,1)S(1)}, bf16[8,2,64,1024]{3,2,1,0:T(8,128)(2,1)}, u32[]{:S(2)}) copy-start(bf16[8,2,64,1024]{3,2,1,0:T(8,128)(2,1)} %get-tuple-element.15.dw_ref) | copy-start | bytes 6291460
